TPU v7x, 32 devices: a whole 2x2x4 slice. The times are simulated.
32 devices in a mesh: sp: 16 (over z, y, x), tp: 2 (over core).
Axes of the slice: x: 2, y: 2, z: 4, core: 2. Of those that a mesh axis runs over, the one named last changes fastest.
Arguments:
- activations: bfloat16 [2048, 2048], P('sp', 'tp'), may hold values from -200 to 200
- norm_gain: float32 [2048], replicated, may hold values from 0.1 to 1.9
- state_proj: bfloat16 [2048, 1024], P(None, 'tp'), may hold values from -0.125 to 0.125
- value_proj: bfloat16 [2048, 1024], P(None, 'tp'), may hold values from -0.125 to 0.125
- post_gate_proj: bfloat16 [2048, 1024], P(None, 'tp'), may hold values from -0.125 to 0.125
- pre_gate_proj: bfloat16 [2048, 1024], P(None, 'tp'), may hold values from -0.125 to 0.125
- input_map: bfloat16 [64, 16, 128], P('tp'), may hold values from -1.5 to 1.5
- output_map: float32 [64, 128, 16], P('tp'), may hold values from -0.5 to 0.5
- skip_gain: float32 [1024], P('tp'), may hold values from -4 to 4
- rotation: float32 [64, 64], P('tp'), may hold values from -3.140625 to 3.140625
- log_decay: float32 [2048, 64], P('sp', 'tp'), may hold values from -1.5 to 0, as said below
- initial_state: float32 [2, 64, 64], P(None, 'tp'), may hold values from -12 to 12
- conv_taps: bfloat16 [3, 1024], P(None, 'tp'), may hold values from -3.5 to 3.5
- state_out: bfloat16 [1024, 2048], P(None, 'tp'), may hold values from -0.125 to 0.125
- conv_out: bfloat16 [1024, 2048], P(None, 'tp'), may hold values from -0.125 to 0.125
Outputs:
- layer_out: bfloat16 [2048, 2048], P('sp', 'tp')
Inputs may be any that keep to these rules, and one draw needn't show every extreme that they name: `log_decay`: every entry is negative.
All inputs are finite; a program needn't handle non-finite values.
Results may differ from a plain program's by a relative error of at most 0.014.
Values may be sent and summed in bfloat16 or wider, within the bound.
A program may use at most 64 MiB of HBM per device.

v0:
```python
import functools

import jax
import jax.numpy as jnp
from jax import lax
from jax.experimental import pallas as pl
from jax.experimental.pallas import tpu as pltpu
from jax.sharding import PartitionSpec as P

EPS = 1e-06
LANES = 128
MESH = pl.DeviceIdType.MESH
F32 = jnp.float32
BF16 = jnp.bfloat16


def minus_expm1(y):
    poly = jnp.ones_like(y)
    for k in range(11, 1, -1):
        poly = 1.0 + poly * y * (1.0 / k)
    return jnp.where(y > -0.5, -y * poly, 1.0 - jnp.exp(y))


def split3(v):
    hi = v.astype(BF16)
    rest = v - hi.astype(F32)
    mid = rest.astype(BF16)
    low = (rest - mid.astype(F32)).astype(BF16)
    return hi, mid, low


def cmul(a, b):
    return a[0] * b[0] - a[1] * b[1], a[0] * b[1] + a[1] * b[0]


def cpow(base, count):
    result = None
    while count:
        if count & 1:
            result = base if result is None else cmul(result, base)
        count >>= 1
        if count:
            base = cmul(base, base)
    return result


def inner_of(n):
    return max(d for d in range(1, n + 1) if n % d == 0 and d * d <= n)


def gelu(x):
    return 0.5 * x * (1.0 + jnp.tanh(0.7978845608028654 * (x + 0.044715 * x * x * x)))


def kernel(
    n,
    x_hbm,
    gain_hbm,
    w0_hbm,
    w1_hbm,
    w2_hbm,
    w3_hbm,
    imap_hbm,
    omap_hbm,
    skip_hbm,
    rot_hbm,
    ld_hbm,
    init_hbm,
    taps_hbm,
    so_hbm,
    co_hbm,
    out_ref,
    x_ref,
    gain_ref,
    imap_ref,
    omap_ref,
    skip_ref,
    rot_ref,
    ld_ref,
    init_ref,
    taps_ref,
    wv,
    ov,
    xr,
    acc,
    din,
    bd_in,
    bd_out,
    map_t,
    tbl,
    powers,
    chan_end,
    chan_gain,
    rowed,
    post,
    table_far,
    map_far,
    post_far,
    aux,
    aux_far,
    held,
    enter,
    sums,
    to_chan,
    mag,
    drv,
    pairs,
    pad,
    near_in,
    far_in,
    far_out,
    hs,
    hc,
    oacc,
    in_sem,
    wsem,
    osem,
    x_sem,
    tail_sem,
    hc_sem,
    hs_sem,
    near_send,
    near_recv,
    far_send,
    far_recv,
    aux_sem,
    enter_sem,
    dup_sem,
    near_ready,
    far_ready,
):
    sp, tp = lax.axis_index("sp"), lax.axis_index("tp")
    other = 1 - tp
    rows, half = x_ref.shape
    groups, state = rot_ref.shape
    gch = imap_ref.shape[1]
    chans = groups * gch
    states = groups * state
    prow = states // LANES
    per_block = LANES // gch
    blocks = groups // per_block
    quads = prow // blocks
    pitch = drv.shape[0] // rows
    bstates = quads * LANES
    cwide = taps_ref.shape[1]
    width = taps_ref.shape[0]

    barrier = pltpu.get_barrier_semaphore()
    partner = {"sp": sp, "tp": other}

    inner = inner_of(n)
    outer = n // inner
    a, b = lax.div(sp, inner), lax.rem(sp, inner)
    last = outer - 1

    hop_on = (b == inner - 1) & (a < last)

    def tell(sem, j):
        for t in (0, 1):
            pl.semaphore_signal(sem, inc=1, device_id={"sp": j, "tp": t}, device_id_type=MESH)

    def greet_near(k, c):
        tell(barrier, a * inner + k)
        return c

    def greet_far(k, c):
        tell(barrier, k * inner + b)
        return c

    pl.semaphore_signal(barrier, inc=1, device_id=partner, device_id_type=MESH)
    lax.fori_loop(b + 1, inner, greet_near, 0)

    lax.fori_loop(a + 1, outer, greet_far, 0)

    in_copies = {}
    def fetch(i, src, dst):
        in_copies[i] = pltpu.make_async_copy(src, dst, in_sem.at[i])
        in_copies[i].start()

    w_hbm = (w0_hbm, w1_hbm, w2_hbm, w3_hbm)

    def fetch_weight(i, h, sem):
        part = (tp, other)[h]
        pltpu.make_async_copy(
            w_hbm[i].at[pl.ds(part * half, half), :], wv.at[i, pl.ds(h * half, half), :], sem
        ).start()

    def wait_weight(i):
        pltpu.make_async_copy(w_hbm[i], wv.at[i], wsem.at[i]).wait()

    fetch(0, x_hbm, x_ref)
    fetch(4, ld_hbm, ld_ref)
    fetch(2, rot_hbm, rot_ref)
    fetch(5, imap_hbm, imap_ref)
    fetch(1, gain_hbm, gain_ref)
    fetch_weight(0, 0, wsem.at[0])
    fetch_weight(0, 1, wsem.at[4])

    pl.semaphore_wait(barrier, 1 + 2 * (b + a))

    def ready_near(k, c):
        tell(near_ready, a * inner + k)
        return c

    def ready_far(k, c):
        tell(far_ready, k * inner + b)
        return c

    @pl.when(tp == 1)
    def _():
        lax.fori_loop(0, b, ready_near, 0)


    lax.fori_loop(0, a, ready_far, 0)

    when = lax.broadcasted_iota(jnp.int32, (rows, 2 * rows), 0)
    upto = lax.broadcasted_iota(jnp.int32, (rows, 2 * rows), 1)
    sums[...] = jnp.where(
        ((upto < rows) & (when <= upto)) | ((upto >= rows) & (when > upto - rows)), 1.0, 0.0
    ).astype(BF16)
    col = lax.broadcasted_iota(jnp.int32, (groups, chans), 1)
    row = lax.broadcasted_iota(jnp.int32, (groups, chans), 0)
    to_chan[...] = jnp.where((col >= row * gch) & (col < (row + 1) * gch), 1.0, 0.0).astype(BF16)

    def remote(src, dst, s, r, dev):
        return pltpu.make_async_remote_copy(
            src_ref=src, dst_ref=dst, send_sem=s, recv_sem=r, device_id=dev, device_id_type=MESH
        )

    in_copies[0].wait()
    x_copy = remote(x_ref, xr, x_sem.at[0], x_sem.at[1], partner)
    x_copy.start()

    fetch(3, init_hbm, init_ref)
    fetch(6, omap_hbm, omap_ref)
    fetch(7, skip_hbm, skip_ref)
    fetch(8, taps_hbm, taps_ref)
    for i in (1, 3, 2):
        for h in (0, 1):
            fetch_weight(i, h, wsem.at[i])
    for i, w, deep in ((1, co_hbm, cwide), (0, so_hbm, chans)):
        for h, part in ((0, tp), (1, other)):
            pltpu.make_async_copy(
                w.at[pl.ds(part * deep, deep), :], ov.at[i, pl.ds(h * deep, deep), :], osem.at[i]
            ).start()

    lane = lax.broadcasted_iota(jnp.int32, (1, LANES), 1)

    def pair_up(i, v):
        pairs[pl.ds(i * groups, groups), :] = v
        even = pairs[pl.ds(i * groups, prow, stride=2), :]
        odd = pairs[pl.ds(i * groups + 1, prow, stride=2), :]
        return jnp.where(lane < state, even, odd)

    def twice(v):
        return jnp.concatenate([v, v], axis=1)

    for i in (4, 2, 5, 1):
        in_copies[i].wait()
    ld = ld_ref[...]

    def time_sums(cols):
        added = jnp.dot(jnp.concatenate(split3(ld), axis=0), sums[:, cols], preferred_element_type=F32)
        return added[:groups] + added[groups : 2 * groups] + added[2 * groups :]

    def per_channel(v):
        hi, mid, _ = split3(v.T)
        return jnp.dot(hi, to_chan[...], preferred_element_type=F32) + jnp.dot(
            mid, to_chan[...], preferred_element_type=F32
        )

    gain = jnp.sqrt(minus_expm1(2.0 * ld))
    chan_end[...] = per_channel(gain * jnp.exp(time_sums(slice(rows, 2 * rows))))
    tot = pair_up(
        3, jnp.broadcast_to(jnp.exp(jnp.sum(ld, axis=1, keepdims=True)), (groups, LANES))
    )
    theta = pair_up(0, twice(rot_ref[...]))
    turn = jnp.cos(theta), jnp.sin(theta)
    step = turn
    for k in range(8):
        for i in (0, 1):
            powers[i, pl.ds(k * prow, prow), :] = step[i]
        step = cmul(step, turn) if k < 7 else step
    far_step16 = cmul(step, step)
    for i in (0, 1):
        powers[i, pl.ds(8 * prow, prow), :] = far_step16[i]
    whole = cpow(step, rows // 8)
    for r in range(prow):
        even = [powers[i, pl.ds(r, 8, stride=prow), :] for i in (0, 1)]
        eight = [powers[i, pl.ds(7 * prow + r, 1), :] for i in (0, 1)]
        sixteen = [powers[i, pl.ds(8 * prow + r, 1), :] for i in (0, 1)]
        odd = cmul(even, eight)
        for t in range(0, rows, 16):
            for i in (0, 1):
                tbl[t : t + 16, (2 * r + i) * LANES : (2 * r + i + 1) * LANES] = jnp.concatenate(
                    [even[i], odd[i]], axis=0
                ).astype(BF16)
            even = cmul(even, sixteen)
            odd = cmul(odd, sixteen)

    def spread_map(src, dst):
        dst[...] = jnp.zeros_like(dst)
        for b in range(blocks):
            for q in range(quads):
                g = b * per_block + 2 * q
                one = src[g].astype(F32)
                two = src[g + 1].astype(F32)
                one_r = jnp.concatenate([one[:, state:], one[:, :state]], axis=1)
                two_r = jnp.concatenate([two[:, state:], two[:, :state]], axis=1)
                low = lane < state
                re = jnp.concatenate([jnp.where(low, one, 0.0), jnp.where(low, 0.0, two_r)], axis=0)
                im = jnp.concatenate([jnp.where(low, one_r, 0.0), jnp.where(low, 0.0, two)], axis=0)
                at = pl.ds(b * LANES + q * 2 * gch, 2 * gch)
                dst[at, 2 * q * LANES : (2 * q + 1) * LANES] = re.astype(BF16)
                dst[at, (2 * q + 1) * LANES : (2 * q + 2) * LANES] = im.astype(BF16)

    spread_map(imap_ref, bd_in)
    own = x_ref[...].astype(F32)
    scaled = (own * gain_ref[:, pl.ds(pl.multiple_of(tp * half, LANES), half)]).astype(BF16)
    squares = jnp.sum(own * own, axis=1, keepdims=True)
    half_copy = pltpu.make_async_copy(w_hbm[0].at[pl.ds(0, half), :], wv.at[0, pl.ds(0, half), :], wsem.at[0])
    half_copy.wait()
    partial = jnp.dot(scaled, wv[0, :half], preferred_element_type=F32)
    acc[:, :half] = scaled

    x_copy.wait_recv()
    far_x = xr[...].astype(F32)
    scaled_far = (far_x * gain_ref[:, pl.ds(pl.multiple_of(other * half, LANES), half)]).astype(BF16)
    squares = squares + jnp.sum(far_x * far_x, axis=1, keepdims=True)
    scale = lax.rsqrt(squares / (2 * half) + EPS)

    acc[:, half:] = scaled_far
    rest_copy = pltpu.make_async_copy(
        w_hbm[0].at[pl.ds(0, half), :], wv.at[0, pl.ds(half, half), :], wsem.at[4]
    )
    rest_copy.wait()
    total = partial + jnp.dot(scaled_far, wv[0, half:], preferred_element_type=F32)
    drive_in = (total * scale).astype(BF16)
    din[...] = drive_in
    ends_in = (drive_in.astype(F32) * chan_end[...]).astype(BF16).T
    for r in range(prow):
        q = r % quads
        at = slice(r * 2 * gch, (r + 1) * 2 * gch)
        seen = jnp.dot(
            ends_in[at], tbl[:, 2 * r * LANES : (2 * r + 2) * LANES], preferred_element_type=F32
        )
        m_re = bd_in[at, 2 * q * LANES : (2 * q + 1) * LANES].astype(F32)
        m_im = bd_in[at, (2 * q + 1) * LANES : (2 * q + 2) * LANES].astype(F32)
        c, d = seen[:, :LANES], seen[:, LANES:]
        rowed[0, r : r + 1, :] = jnp.sum(c * m_re + d * m_im, axis=0, keepdims=True)
        rowed[1, r : r + 1, :] = jnp.sum(c * m_im - d * m_re, axis=0, keepdims=True)
    e_re, e_im = cmul(whole, (rowed[0], rowed[1]))

    near_in[tp, b, pl.ds(0, prow), :] = e_re.astype(BF16)
    near_in[tp, b, pl.ds(prow, prow), :] = e_im.astype(BF16)
    fore = lax.rem(lax.broadcasted_iota(jnp.int32, (prow, LANES), 1), state) < state // 2

    def packed(v):
        hi, mid, _ = split3(v)
        return jnp.where(fore, hi.astype(F32), mid.astype(F32)).astype(BF16)

    near_in[tp, b, pl.ds(2 * prow, prow), :] = packed(tot)

    def near_copy(k):
        return remote(
            near_in.at[tp, b],
            near_in.at[tp, b],
            near_send.at[k],
            near_recv.at[tp, b],
            {"sp": a * inner + k, "tp": 1},
        )

    def far_copy(k):
        return remote(
            far_out, far_in.at[a], far_send.at[k], far_recv.at[a], {"sp": k * inner + b, "tp": 1}
        )

    near_from = jnp.where(a < last, 0, b + 1)
    near_upto = jnp.where(a < last, inner, b)
    after = inner - 1 - b

    @pl.when(after > 0)
    def _():
        pl.semaphore_wait(near_ready, after)

    def send_near(k, c):
        @pl.when((k != b) | ((tp == 0) & (a < last)))
        def _():
            near_copy(k).start()

        return c

    lax.fori_loop(near_from, inner, send_near, 0)

    in_copies[3].wait()
    aux[0], aux[1] = whole
    aux[2] = pair_up(1, twice(init_ref[0]))
    aux[3] = pair_up(2, twice(init_ref[1]))
    aux_copy = remote(aux, aux_far, aux_sem.at[0], aux_sem.at[1], partner)
    dup_copies = [
        remote(src, dst, dup_sem.at[0, i], dup_sem.at[1, i], partner)
        for i, (src, dst) in enumerate(((tbl, table_far), (map_t, map_far), (post, post_far)))
    ]

    def give(copy):
        @pl.when(tp == 0)
        def _():
            copy.start()

    give(aux_copy)

    def project(i):
        wait_weight(i)
        total = jnp.dot(acc[...], wv[i], preferred_element_type=F32)
        return (total * scale).astype(BF16)

    value = project(1)
    pre_gate = project(3)
    mixed = (pre_gate.astype(F32) * value.astype(F32)).astype(BF16).astype(F32)
    pad[pl.ds(8, rows), :] = mixed
    tail_copy = remote(
        pad.at[pl.ds(rows, 8), :],
        pad.at[pl.ds(0, 8), :],
        tail_sem.at[0],
        tail_sem.at[1],
        {"sp": lax.rem(sp + 1, n), "tp": tp},
    )

    @pl.when(hop_on)
    def _():
        pl.semaphore_wait(far_ready, 2 * (last - a))

    @pl.when(sp < n - 1)
    def _():
        tail_copy.start()

    give(dup_copies[0])

    for i in (6, 7):
        in_copies[i].wait()
    spread_map(omap_ref, bd_out)
    for k in range(blocks):
        map_t[2 * k * bstates : 2 * (k + 1) * bstates, :] = bd_out[k * LANES : (k + 1) * LANES, :].T
    give(dup_copies[1])

    ld = ld_ref[...]
    gain = jnp.sqrt(minus_expm1(2.0 * ld))
    late = per_channel(jnp.concatenate([jnp.exp(time_sums(slice(0, rows))), gain], axis=1))
    post[1] = late[:rows]
    chan_gain[...] = late[rows:]
    mags = split3(jnp.exp(ld).T)[:2]
    for k in range(blocks):
        col = lax.broadcasted_iota(jnp.int32, (groups, bstates), 1) + k * bstates
        row = lax.broadcasted_iota(jnp.int32, (groups, bstates), 0)
        spread = jnp.where(
            (col >= row * state) & (col < (row + 1) * state), 1.0, 0.0
        ).astype(BF16)
        m = jnp.dot(mags[0], spread, preferred_element_type=F32) + jnp.dot(
            mags[1], spread, preferred_element_type=F32
        )
        for q in range(quads):
            mag[pl.ds(k * quads + q, rows, stride=prow), :] = m[:, q * LANES : (q + 1) * LANES]

    hc[0] = project(2)
    gained = (din[...].astype(F32) * chan_gain[...]).astype(BF16)
    for k in range(blocks):
        blk = jnp.dot(
            gained[:, k * LANES : (k + 1) * LANES],
            bd_in[k * LANES : (k + 1) * LANES, :],
            preferred_element_type=F32,
        )
        for q in range(quads):
            r = k * quads + q
            drv[pl.ds(r, rows, stride=pitch), :] = blk[:, 2 * q * LANES : (2 * q + 1) * LANES]
            drv[pl.ds(prow + r, rows, stride=pitch), :] = blk[
                :, (2 * q + 1) * LANES : (2 * q + 2) * LANES
            ]

    zero = jnp.zeros((prow, LANES), F32)

    def message(ref):
        v = ref[pl.ds(2 * prow, prow), :].astype(F32)
        mags = v + jnp.where(fore, pltpu.roll(v, LANES - state // 2, 1), pltpu.roll(v, state // 2, 1))
        return ref[pl.ds(0, prow), :].astype(F32), ref[pl.ds(prow, prow), :].astype(F32), mags

    def send_far(k, c):
        far_copy(outer + a - k).start()
        return c

    def join_half(h, turned, first):
        def near_step(k, c):
            @pl.when((k != b) | (h == 0))
            def _():
                remote(
                    near_in.at[h, k],
                    near_in.at[h, k],
                    near_send.at[k],
                    near_recv.at[h, k],
                    {"sp": a * inner + k, "tp": 0},
                ).wait_recv()

            ends, mag_all, phase, mine = c[0:2], c[2], c[3:5], c[5:]
            k_re, k_im, k_mag = message(near_in.at[h, k])
            moved = cmul((turned[0] * k_mag, turned[1] * k_mag), ends)
            now = (moved[0] + k_re, moved[1] + k_im, mag_all * k_mag) + cmul(turned, phase)
            return now + tuple(jnp.where(k < b, v, w) for v, w in zip(now, mine))

        one = jnp.ones((prow, LANES), F32)
        begin = tuple(jnp.where(a == 0, v, zero) for v in first) + (one, one, zero)
        plane = lax.fori_loop(0, near_upto, near_step, begin + begin)
        for i in range(5):
            held[h, i] = plane[5 + i]
        far_out[h, pl.ds(0, prow), :] = plane[0].astype(BF16)
        far_out[h, pl.ds(prow, prow), :] = plane[1].astype(BF16)
        far_out[h, pl.ds(2 * prow, prow), :] = packed(plane[2])

    def join_near():
        @pl.when(tp == 1)
        def _():
            join_half(1, whole, (aux[2], aux[3]))
            join_half(0, (aux_far[0], aux_far[1]), (aux_far[2], aux_far[3]))

        @pl.when((a < last) & (b < inner - 1))
        def _():
            pl.semaphore_wait(far_ready, 2 * (last - a))

        @pl.when((tp == 1) & (a < last))
        def _():
            lax.fori_loop(a + 1, outer, send_far, 0)

    @pl.when(tp == 1)
    def _():
        aux_copy.wait_recv()

    @pl.when(b > 0)
    def _():
        join_near()

    def scan(t, h):
        m = mag[pl.ds(pl.multiple_of(t * prow, prow), prow), :]
        base = pl.multiple_of(t * pitch, 8)
        d_re = drv[pl.ds(base, prow), :]
        d_im = drv[pl.ds(base + prow, prow), :]
        f_re, f_im = m * turn[0], m * turn[1]
        new_re = (f_re * h[0] + d_re) - f_im * h[1]
        new_im = (f_re * h[1] + d_im) + f_im * h[0]
        drv[pl.ds(base, prow), :] = new_re
        drv[pl.ds(base + prow, prow), :] = new_im
        return new_re, new_im

    lax.fori_loop(0, rows, scan, (zero, zero), unroll=8)
    for k in range(blocks):
        cols = slice(k * LANES, (k + 1) * LANES)
        at = [half_row + k * quads + q for q in range(quads) for half_row in (0, prow)]
        st = jnp.concatenate(
            [drv[pl.ds(r, rows, stride=pitch), :].astype(BF16) for r in at], axis=1
        )
        read = jnp.dot(
            st, map_t[2 * k * bstates : 2 * (k + 1) * bstates, :], preferred_element_type=F32
        )
        post[0, :, cols] = read + skip_ref[:, cols] * din[:, cols].astype(F32)

    give(dup_copies[2])

    @pl.when(b == 0)
    def _():
        join_near()

    @pl.when(sp == 0)
    def _():
        pad[pl.ds(0, 8), :] = jnp.zeros((8, cwide), F32)

    in_copies[8].wait()

    @pl.when(sp > 0)
    def _():
        tail_copy.wait_recv()

    conv = jnp.zeros((rows, cwide), F32)
    for k in range(width):
        conv = conv + pad[pl.ds(8 + k - (width - 1), rows), :] * taps_ref[k : k + 1, :].astype(F32)
    hc[0] = (hc[0].astype(F32) * conv).astype(BF16)
    hc_copy = remote(hc.at[0], hc.at[1], hc_sem.at[0], hc_sem.at[1], partner)
    hc_copy.start()
    for i in (0, 1):
        pltpu.make_async_copy((so_hbm, co_hbm)[i], ov.at[i], osem.at[i]).wait()
    oacc[...] = jnp.dot(hc[0], ov[1, :cwide], preferred_element_type=F32)
    hc_copy.wait_recv()
    oacc[...] += jnp.dot(hc[1], ov[1, cwide:], preferred_element_type=F32)
    def entering(h, turned):
        plane_turn = cpow(turned, inner)

        def far_step(k, c):
            k_re, k_im, k_mag = message(far_in.at[k, h])
            moved = cmul((plane_turn[0] * k_mag, plane_turn[1] * k_mag), c)
            return moved[0] + k_re, moved[1] + k_im

        before = lax.fori_loop(0, a, far_step, (zero, zero))
        moved = cmul((held[h, 3] * held[h, 2], held[h, 4] * held[h, 2]), before)
        return held[h, 0] + moved[0], held[h, 1] + moved[1]

    def correct(h, table, mapped, local, slot):
        moved = []
        for k in range(blocks):
            turned = []
            for r in range(k * quads, (k + 1) * quads):
                c, d = (
                    table[:, (2 * r + i) * LANES : (2 * r + i + 1) * LANES].reshape(rows // 16, 16, LANES)
                    for i in (0, 1)
                )
                h_re, h_im = (
                    jnp.broadcast_to(enter[h, i, r : r + 1, :], (16, LANES)).astype(BF16)[None]
                    for i in (0, 1)
                )
                turned += cmul((c, d), (h_re, h_im))
            moved.append(
                jnp.dot(
                    jnp.concatenate([v.reshape(rows, LANES) for v in turned], axis=1),
                    mapped[2 * k * bstates : 2 * (k + 1) * bstates, :],
                    preferred_element_type=F32,
                )
            )
        for k in range(blocks):
            cols = slice(k * LANES, (k + 1) * LANES)
            hs[slot, :, cols] = gelu(local[0, :, cols] + local[1, :, cols] * moved[k]).astype(BF16)

    def far_arrival(k, c):
        far_from = remote(
            far_in.at[k], far_in.at[k], far_send.at[k], far_recv.at[k], {"sp": k * inner + b, "tp": 0}
        )
        far_from.wait_recv()
        return c

    enter_copy = remote(enter.at[0], enter.at[0], enter_sem.at[0], enter_sem.at[1], partner)

    @pl.when(tp == 1)
    def _():
        lax.fori_loop(0, a, far_arrival, 0)
        enter[0, 0], enter[0, 1] = entering(0, (aux_far[0], aux_far[1]))
        enter_copy.start()
        enter[1, 0], enter[1, 1] = entering(1, whole)

    @pl.when(tp == 0)
    def _():
        enter_copy.wait_recv()

    correct(tp, tbl, map_t, post, 0)
    hs_copy = remote(hs.at[0], hs.at[1], hs_sem.at[0], hs_sem.at[1], partner)

    @pl.when(tp == 1)
    def _():
        hs_copy.start()
        for copy in dup_copies:
            copy.wait_recv()
        correct(0, table_far, map_far, post_far, 1)

    oacc[...] += jnp.dot(hs[0], ov[0, :chans], preferred_element_type=F32)

    @pl.when(tp == 0)
    def _():
        hs_copy.wait_recv()

    out_ref[...] = (oacc[...] + jnp.dot(hs[1], ov[0, chans:], preferred_element_type=F32)).astype(BF16)

    x_copy.wait_send()
    hc_copy.wait_send()

    @pl.when(tp == 1)
    def _():
        hs_copy.wait_send()
        enter_copy.wait_send()

    @pl.when(tp == 0)
    def _():
        aux_copy.wait_send()
        for copy in dup_copies:
            copy.wait_send()

    @pl.when(sp < n - 1)
    def _():
        tail_copy.wait_send()

    def near_sent(k, c):
        @pl.when((k != b) | ((tp == 0) & (a < last)))
        def _():
            near_copy(k).wait_send()

        return c

    def far_sent(k, c):
        far_copy(k).wait_send()
        return c

    lax.fori_loop(near_from, inner, near_sent, 0)

    @pl.when(tp == 1)
    def _():
        lax.fori_loop(a + 1, outer, far_sent, 0)


def on_device(
    activations,
    norm_gain,
    state_proj,
    value_proj,
    post_gate_proj,
    pre_gate_proj,
    input_map,
    output_map,
    skip_gain,
    rotation,
    log_decay,
    initial_state,
    conv_taps,
    state_out,
    conv_out,
):
    n = lax.axis_size("sp")
    rows, half = activations.shape
    groups, state = rotation.shape
    chans = state_proj.shape[1]
    cwide = value_proj.shape[1]
    outs = state_out.shape[1]
    states = groups * state
    prow = states // LANES
    inner = inner_of(n)
    bdw = 2 * states // (chans // LANES)
    vmem = pl.BlockSpec(memory_space=pltpu.VMEM)
    hbm = pl.BlockSpec(memory_space=pl.ANY)
    dma = pltpu.SemaphoreType.DMA
    return pl.pallas_call(
        functools.partial(kernel, n),
        out_shape=pltpu.VMEM((rows, outs), BF16),
        in_specs=[hbm] * 15,
        out_specs=vmem,
        scratch_shapes=[
            pltpu.VMEM((rows, half), BF16),
            pltpu.VMEM((1, 2 * half), F32),
            pltpu.VMEM(input_map.shape, BF16),
            pltpu.VMEM((groups, output_map.shape[2], output_map.shape[1]), F32),
            pltpu.VMEM((1, chans), F32),
            pltpu.VMEM((groups, state), F32),
            pltpu.VMEM((groups, rows), F32),
            pltpu.VMEM(initial_state.shape, F32),
            pltpu.VMEM(conv_taps.shape, BF16),
            pltpu.VMEM((4, 2 * half, chans), BF16),
            pltpu.VMEM((2, 2 * chans, outs), BF16),
            pltpu.VMEM((rows, half), BF16),
            pltpu.VMEM((rows, 2 * half), BF16),
            pltpu.VMEM((rows, chans), BF16),
            pltpu.VMEM((chans, bdw), BF16),
            pltpu.VMEM((chans, bdw), BF16),
            pltpu.VMEM((2 * states, LANES), BF16),
            pltpu.VMEM((rows, 2 * states), BF16),
            pltpu.VMEM((2, 9 * prow, LANES), F32),
            pltpu.VMEM((rows, chans), F32),
            pltpu.VMEM((rows, chans), F32),
            pltpu.VMEM((2, prow, LANES), F32),
            pltpu.VMEM((2, rows, chans), F32),
            pltpu.VMEM((rows, 2 * states), BF16),
            pltpu.VMEM((2 * states, LANES), BF16),
            pltpu.VMEM((2, rows, chans), F32),
            pltpu.VMEM((4, prow, LANES), F32),
            pltpu.VMEM((4, prow, LANES), F32),
            pltpu.VMEM((2, 5, prow, LANES), F32),
            pltpu.VMEM((2, 2, prow, LANES), F32),
            pltpu.VMEM((rows, 2 * rows), BF16),
            pltpu.VMEM((groups, chans), BF16),
            pltpu.VMEM((rows * prow, LANES), F32),
            pltpu.VMEM((rows * (2 * prow + 8), LANES), F32),
            pltpu.VMEM((4 * groups, LANES), F32),
            pltpu.VMEM((rows + 8, cwide), F32),
            pltpu.VMEM((2, inner, 3 * prow, LANES), BF16),
            pltpu.VMEM((n // inner, 2, 3 * prow, LANES), BF16),
            pltpu.VMEM((2, 3 * prow, LANES), BF16),
            pltpu.VMEM((2, rows, chans), BF16),
            pltpu.VMEM((2, rows, cwide), BF16),
            pltpu.VMEM((rows, outs), F32),
            dma((9,)),
            dma((5,)),
            dma((2,)),
            dma((2,)),
            dma((2,)),
            dma((2,)),
            dma((2,)),
            dma((inner,)),
            dma((2, inner)),
            dma((n // inner,)),
            dma((n // inner,)),
            dma((2,)),
            dma((2,)),
            dma((2, 3)),
            pltpu.SemaphoreType.REGULAR,
            pltpu.SemaphoreType.REGULAR,
        ],
        compiler_params=pltpu.CompilerParams(collective_id=0, has_side_effects=True),
    )(
        activations,
        norm_gain.reshape(1, -1),
        state_proj,
        value_proj,
        post_gate_proj,
        pre_gate_proj,
        input_map,
        jnp.swapaxes(output_map, 1, 2),
        skip_gain.reshape(1, -1),
        rotation,
        jnp.swapaxes(log_decay, 0, 1),
        initial_state,
        conv_taps,
        state_out,
        conv_out,
    )


def solution(mesh):
    return jax.shard_map(
        on_device,
        mesh=mesh,
        in_specs=(
            P("sp", "tp"),
            P(),
            P(None, "tp"),
            P(None, "tp"),
            P(None, "tp"),
            P(None, "tp"),
            P("tp", None, None),
            P("tp", None, None),
            P("tp"),
            P("tp", None),
            P("sp", "tp"),
            P(None, "tp", None),
            P(None, "tp"),
            P(None, "tp"),
            P(None, "tp"),
        ),
        out_specs=P("sp", "tp"),
        check_vma=False,
    )
```

profile of v0, /device:TPU:0, one launch (start us, length us, event | category | flops | bytes accessed | tf_op | source)
XLA Modules:
  0.0 13.9 jit_solution(17181576258913107784)
XLA Ops:
  0.0 13.1 %shard_map.145 = bf16[128,1024]{1,0:T(8,128)(2,1)S(1)} custom-call(bf16[128,1024]{1,0:T(8,128)(2,1)} %x_hbm.1, f32[1,2048]{1,0:T(1,128)} %bitcast.6, bf16[2048,512]{1,0:T(8,128)(2,1)} %w0_hbm.1, bf16[2048,512]{1,0:T(8,128)(2,1)} %w1_hbm.1, bf16[2048,512]{1,0:T(8,128)(2,1)} %w2_hbm.1, bf16[2048,512]{1,0:T(8,128)(2,1)} %w3_hbm.1, ...), custom_call_target="tpu_custom_call" | custom-call | tf_op jit(solution)/shard_map/pallas_call | solution.py:731
  13.2 0.7 %copy.17 = bf16[128,1024]{1,0:T(8,128)(2,1)} copy(bf16[128,1024]{1,0:T(8,128)(2,1)S(1)} %shard_map.145) | data formatting | bytes 524288
where the time goes:
time: 14 us; the launch traced here: 13.9 us
  Pallas kernels  13.1 us (94%)
  local copies, waits for them, and re-layouts  0.71 us (5%)
    pallas_call x1, Pallas kernels, on_device(): pl.pallas_call(functools.partial(kernel, n), out_shape=pltpu.VMEM((rows,...  13.1 us
    unnamed x1, local copies, waits for them, and re-layouts  0.71 us

commit v1 on v0

--- a/solution.py
+++ b/solution.py
@@ -98,6 +98,7 @@
     post_far,
     aux,
     aux_far,
+    mags_in,
     held,
     enter,
     sums,
@@ -399,7 +400,14 @@
     aux_copy = remote(aux, aux_far, aux_sem.at[0], aux_sem.at[1], partner)
     dup_copies = [
         remote(src, dst, dup_sem.at[0, i], dup_sem.at[1, i], partner)
-        for i, (src, dst) in enumerate(((tbl, table_far), (map_t, map_far), (post, post_far)))
+        for i, (src, dst) in enumerate(
+            (
+                (tbl, table_far),
+                (map_t, map_far),
+                (post.at[1], post_far.at[1]),
+                (post.at[0], post_far.at[0]),
+            )
+        )
     ]
 
     def give(copy):
@@ -447,6 +455,7 @@
     gain = jnp.sqrt(minus_expm1(2.0 * ld))
     late = per_channel(jnp.concatenate([jnp.exp(time_sums(slice(0, rows))), gain], axis=1))
     post[1] = late[:rows]
+    give(dup_copies[2])
     chan_gain[...] = late[rows:]
     mags = split3(jnp.exp(ld).T)[:2]
     for k in range(blocks):
@@ -461,34 +470,30 @@
         for q in range(quads):
             mag[pl.ds(k * quads + q, rows, stride=prow), :] = m[:, q * LANES : (q + 1) * LANES]
 
-    hc[0] = project(2)
-    gained = (din[...].astype(F32) * chan_gain[...]).astype(BF16)
-    for k in range(blocks):
-        blk = jnp.dot(
-            gained[:, k * LANES : (k + 1) * LANES],
-            bd_in[k * LANES : (k + 1) * LANES, :],
-            preferred_element_type=F32,
-        )
-        for q in range(quads):
-            r = k * quads + q
-            drv[pl.ds(r, rows, stride=pitch), :] = blk[:, 2 * q * LANES : (2 * q + 1) * LANES]
-            drv[pl.ds(prow + r, rows, stride=pitch), :] = blk[
-                :, (2 * q + 1) * LANES : (2 * q + 2) * LANES
-            ]
-
     zero = jnp.zeros((prow, LANES), F32)
 
-    def message(ref):
-        v = ref[pl.ds(2 * prow, prow), :].astype(F32)
-        mags = v + jnp.where(fore, pltpu.roll(v, LANES - state // 2, 1), pltpu.roll(v, state // 2, 1))
-        return ref[pl.ds(0, prow), :].astype(F32), ref[pl.ds(prow, prow), :].astype(F32), mags
+    def unpacked(v):
+        v = v.astype(F32)
+        keep = lax.rem(lax.broadcasted_iota(jnp.int32, v.shape, 1), state) < state // 2
+        return v + jnp.where(keep, pltpu.roll(v, LANES - state // 2, 1), pltpu.roll(v, state // 2, 1))
+
+    def unpack_all(ref, h, count, index):
+        packs = jnp.concatenate([ref[index(h, k) + (pl.ds(2 * prow, prow),)] for k in range(count)], axis=0)
+        mags_in[h, : count * prow, :] = unpacked(packs)
+
+    def message(ref, h, k):
+        return (
+            ref[pl.ds(0, prow), :].astype(F32),
+            ref[pl.ds(prow, prow), :].astype(F32),
+            mags_in[h, pl.ds(pl.multiple_of(k * prow, prow), prow), :],
+        )
 
     def send_far(k, c):
         far_copy(outer + a - k).start()
         return c
 
-    def join_half(h, turned, first):
-        def near_step(k, c):
+    def near_arrival(h):
+        def arrival(k, c):
             @pl.when((k != b) | (h == 0))
             def _():
                 remote(
@@ -499,8 +504,16 @@
                     {"sp": a * inner + k, "tp": 0},
                 ).wait_recv()
 
+            return c
+
+        lax.fori_loop(0, near_upto, arrival, 0)
+
+    def join_half(h, turned, first):
+        unpack_all(near_in, h, inner, lambda h, k: (h, k))
+
+        def near_step(k, c):
             ends, mag_all, phase, mine = c[0:2], c[2], c[3:5], c[5:]
-            k_re, k_im, k_mag = message(near_in.at[h, k])
+            k_re, k_im, k_mag = message(near_in.at[h, k], h, k)
             moved = cmul((turned[0] * k_mag, turned[1] * k_mag), ends)
             now = (moved[0] + k_re, moved[1] + k_im, mag_all * k_mag) + cmul(turned, phase)
             return now + tuple(jnp.where(k < b, v, w) for v, w in zip(now, mine))
@@ -517,6 +530,8 @@
     def join_near():
         @pl.when(tp == 1)
         def _():
+            near_arrival(1)
+            near_arrival(0)
             join_half(1, whole, (aux[2], aux[3]))
             join_half(0, (aux_far[0], aux_far[1]), (aux_far[2], aux_far[3]))
 
@@ -532,7 +547,26 @@
     def _():
         aux_copy.wait_recv()
 
-    @pl.when(b > 0)
+    @pl.when(b > 1)
+    def _():
+        join_near()
+
+    hc[0] = project(2)
+    gained = (din[...].astype(F32) * chan_gain[...]).astype(BF16)
+    for k in range(blocks):
+        blk = jnp.dot(
+            gained[:, k * LANES : (k + 1) * LANES],
+            bd_in[k * LANES : (k + 1) * LANES, :],
+            preferred_element_type=F32,
+        )
+        for q in range(quads):
+            r = k * quads + q
+            drv[pl.ds(r, rows, stride=pitch), :] = blk[:, 2 * q * LANES : (2 * q + 1) * LANES]
+            drv[pl.ds(prow + r, rows, stride=pitch), :] = blk[
+                :, (2 * q + 1) * LANES : (2 * q + 2) * LANES
+            ]
+
+    @pl.when(b == 1)
     def _():
         join_near()
 
@@ -560,7 +594,9 @@
         )
         post[0, :, cols] = read + skip_ref[:, cols] * din[:, cols].astype(F32)
 
-    give(dup_copies[2])
+    @pl.when(b == 0)
+    def _():
+        give(dup_copies[3])
 
     @pl.when(b == 0)
     def _():
@@ -582,16 +618,30 @@
     hc[0] = (hc[0].astype(F32) * conv).astype(BF16)
     hc_copy = remote(hc.at[0], hc.at[1], hc_sem.at[0], hc_sem.at[1], partner)
     hc_copy.start()
+
+    @pl.when(b > 0)
+    def _():
+        give(dup_copies[3])
+
     for i in (0, 1):
         pltpu.make_async_copy((so_hbm, co_hbm)[i], ov.at[i], osem.at[i]).wait()
     oacc[...] = jnp.dot(hc[0], ov[1, :cwide], preferred_element_type=F32)
-    hc_copy.wait_recv()
-    oacc[...] += jnp.dot(hc[1], ov[1, cwide:], preferred_element_type=F32)
+
+    def add_far_conv():
+        hc_copy.wait_recv()
+        oacc[...] += jnp.dot(hc[1], ov[1, cwide:], preferred_element_type=F32)
+
+    @pl.when(b > 0)
+    def _():
+        add_far_conv()
+
     def entering(h, turned):
         plane_turn = cpow(turned, inner)
 
+        unpack_all(far_in, h, last, lambda h, k: (k, h))
+
         def far_step(k, c):
-            k_re, k_im, k_mag = message(far_in.at[k, h])
+            k_re, k_im, k_mag = message(far_in.at[k, h], h, k)
             moved = cmul((plane_turn[0] * k_mag, plane_turn[1] * k_mag), c)
             return moved[0] + k_re, moved[1] + k_im
 
@@ -655,6 +705,10 @@
         correct(0, table_far, map_far, post_far, 1)
 
     oacc[...] += jnp.dot(hs[0], ov[0, :chans], preferred_element_type=F32)
+
+    @pl.when(b == 0)
+    def _():
+        add_far_conv()
 
     @pl.when(tp == 0)
     def _():
@@ -762,6 +816,7 @@
             pltpu.VMEM((2, rows, chans), F32),
             pltpu.VMEM((4, prow, LANES), F32),
             pltpu.VMEM((4, prow, LANES), F32),
+            pltpu.VMEM((2, max(inner, n // inner) * prow, LANES), F32),
             pltpu.VMEM((2, 5, prow, LANES), F32),
             pltpu.VMEM((2, 2, prow, LANES), F32),
             pltpu.VMEM((rows, 2 * rows), BF16),
@@ -789,7 +844,7 @@
             dma((n // inner,)),
             dma((2,)),
             dma((2,)),
-            dma((2, 3)),
+            dma((2, 4)),
             pltpu.SemaphoreType.REGULAR,
             pltpu.SemaphoreType.REGULAR,
         ],

time: 14 us -> 13.4 us (0.957)
  the two profiles are of different devices: /device:TPU:0 before, /device:TPU:25 now
where the time goes in v1:
time: 13.4 us; the launch traced here: 13.1 us
  Pallas kernels  12.4 us (93%)
  local copies, waits for them, and re-layouts  0.71 us (5%)
    pallas_call x1, Pallas kernels, on_device(): pl.pallas_call(functools.partial(kernel, n), out_shape=pltpu.VMEM((rows,...  12.4 us
    unnamed x1, local copies, waits for them, and re-layouts  0.71 us

profile of v1, /device:TPU:25, one launch (start us, length us, event | category | flops | bytes accessed | tf_op | source)
XLA Modules:
  0.0 13.1 jit_solution(15483323483650906127)
XLA Ops:
  0.0 12.4 %shard_map.145 = bf16[128,1024]{1,0:T(8,128)(2,1)S(1)} custom-call(bf16[128,1024]{1,0:T(8,128)(2,1)} %x_hbm.1, f32[1,2048]{1,0:T(1,128)} %bitcast.6, bf16[2048,512]{1,0:T(8,128)(2,1)} %w0_hbm.1, bf16[2048,512]{1,0:T(8,128)(2,1)} %w1_hbm.1, bf16[2048,512]{1,0:T(8,128)(2,1)} %w2_hbm.1, bf16[2048,512]{1,0:T(8,128)(2,1)} %w3_hbm.1, ...), custom_call_target="tpu_custom_call" | custom-call | tf_op jit(solution)/shard_map/pallas_call | solution.py:785
  12.4 0.7 %copy.17 = bf16[128,1024]{1,0:T(8,128)(2,1)} copy(bf16[128,1024]{1,0:T(8,128)(2,1)S(1)} %shard_map.145) | data formatting | bytes 524288

commit v2 on v1

--- a/solution.py
+++ b/solution.py
@@ -120,10 +120,8 @@
     tail_sem,
     hc_sem,
     hs_sem,
-    near_send,
-    near_recv,
-    far_send,
-    far_recv,
+    near_sem,
+    far_sem,
     aux_sem,
     enter_sem,
     dup_sem,
@@ -195,7 +193,7 @@
     fetch(5, imap_hbm, imap_ref)
     fetch(1, gain_hbm, gain_ref)
     fetch_weight(0, 0, wsem.at[0])
-    fetch_weight(0, 1, wsem.at[4])
+    fetch_weight(0, 1, wsem.at[0])
 
     pl.semaphore_wait(barrier, 1 + 2 * (b + a))
 
@@ -242,7 +240,7 @@
     for i, w, deep in ((1, co_hbm, cwide), (0, so_hbm, chans)):
         for h, part in ((0, tp), (1, other)):
             pltpu.make_async_copy(
-                w.at[pl.ds(part * deep, deep), :], ov.at[i, pl.ds(h * deep, deep), :], osem.at[i]
+                w.at[pl.ds(part * deep, deep), :], ov.at[pl.ds(2 * i * chans + h * deep, deep), :], osem.at[0]
             ).start()
 
     lane = lax.broadcasted_iota(jnp.int32, (1, LANES), 1)
@@ -319,8 +317,7 @@
     own = x_ref[...].astype(F32)
     scaled = (own * gain_ref[:, pl.ds(pl.multiple_of(tp * half, LANES), half)]).astype(BF16)
     squares = jnp.sum(own * own, axis=1, keepdims=True)
-    half_copy = pltpu.make_async_copy(w_hbm[0].at[pl.ds(0, half), :], wv.at[0, pl.ds(0, half), :], wsem.at[0])
-    half_copy.wait()
+    wait_weight(0)
     partial = jnp.dot(scaled, wv[0, :half], preferred_element_type=F32)
     acc[:, :half] = scaled
 
@@ -331,10 +328,6 @@
     scale = lax.rsqrt(squares / (2 * half) + EPS)
 
     acc[:, half:] = scaled_far
-    rest_copy = pltpu.make_async_copy(
-        w_hbm[0].at[pl.ds(0, half), :], wv.at[0, pl.ds(half, half), :], wsem.at[4]
-    )
-    rest_copy.wait()
     total = partial + jnp.dot(scaled_far, wv[0, half:], preferred_element_type=F32)
     drive_in = (total * scale).astype(BF16)
     din[...] = drive_in
@@ -362,18 +355,26 @@
 
     near_in[tp, b, pl.ds(2 * prow, prow), :] = packed(tot)
 
+    def wait_many(ref, sems, count, upto, sent):
+        for j in range(1, upto + 1):
+            @pl.when(count == j)
+            def _():
+                part = ref.at[pl.ds(0, j)]
+                copy = remote(part, part, sems[0], sems[1], partner)
+                copy.wait_send() if sent else copy.wait_recv()
+
     def near_copy(k):
         return remote(
             near_in.at[tp, b],
             near_in.at[tp, b],
-            near_send.at[k],
-            near_recv.at[tp, b],
+            near_sem.at[2],
+            near_sem.at[tp],
             {"sp": a * inner + k, "tp": 1},
         )
 
     def far_copy(k):
         return remote(
-            far_out, far_in.at[a], far_send.at[k], far_recv.at[a], {"sp": k * inner + b, "tp": 1}
+            far_out, far_in.at[a], far_sem.at[0], far_sem.at[1], {"sp": k * inner + b, "tp": 1}
         )
 
     near_from = jnp.where(a < last, 0, b + 1)
@@ -399,7 +400,7 @@
     aux[3] = pair_up(2, twice(init_ref[1]))
     aux_copy = remote(aux, aux_far, aux_sem.at[0], aux_sem.at[1], partner)
     dup_copies = [
-        remote(src, dst, dup_sem.at[0, i], dup_sem.at[1, i], partner)
+        remote(src, dst, dup_sem.at[0, min(i, 2)], dup_sem.at[1, min(i, 2)], partner)
         for i, (src, dst) in enumerate(
             (
                 (tbl, table_far),
@@ -414,6 +415,10 @@
         @pl.when(tp == 0)
         def _():
             copy.start()
+
+    waited = dup_copies[:2] + [
+        remote(post, post_far, dup_sem.at[0, 2], dup_sem.at[1, 2], partner)
+    ]
 
     give(aux_copy)
 
@@ -492,22 +497,6 @@
         far_copy(outer + a - k).start()
         return c
 
-    def near_arrival(h):
-        def arrival(k, c):
-            @pl.when((k != b) | (h == 0))
-            def _():
-                remote(
-                    near_in.at[h, k],
-                    near_in.at[h, k],
-                    near_send.at[k],
-                    near_recv.at[h, k],
-                    {"sp": a * inner + k, "tp": 0},
-                ).wait_recv()
-
-            return c
-
-        lax.fori_loop(0, near_upto, arrival, 0)
-
     def join_half(h, turned, first):
         unpack_all(near_in, h, inner, lambda h, k: (h, k))
 
@@ -530,8 +519,14 @@
     def join_near():
         @pl.when(tp == 1)
         def _():
-            near_arrival(1)
-            near_arrival(0)
+            for h in (1, 0):
+                wait_many(
+                    near_in.at[h],
+                    (near_sem.at[2], near_sem.at[h]),
+                    jnp.where(a < last, inner - h, b),
+                    inner,
+                    False,
+                )
             join_half(1, whole, (aux[2], aux[3]))
             join_half(0, (aux_far[0], aux_far[1]), (aux_far[2], aux_far[3]))
 
@@ -569,6 +564,29 @@
     @pl.when(b == 1)
     def _():
         join_near()
+
+    hc_copy = remote(hc.at[0], hc.at[1], hc_sem.at[0], hc_sem.at[1], partner)
+
+    def convolve():
+        @pl.when(sp == 0)
+        def _():
+            pad[pl.ds(0, 8), :] = jnp.zeros((8, cwide), F32)
+
+        in_copies[8].wait()
+
+        @pl.when(sp > 0)
+        def _():
+            tail_copy.wait_recv()
+
+        conv = jnp.zeros((rows, cwide), F32)
+        for k in range(width):
+            conv = conv + pad[pl.ds(8 + k - (width - 1), rows), :] * taps_ref[k : k + 1, :].astype(F32)
+        hc[0] = (hc[0].astype(F32) * conv).astype(BF16)
+        hc_copy.start()
+
+    @pl.when(b > 0)
+    def _():
+        convolve()
 
     def scan(t, h):
         m = mag[pl.ds(pl.multiple_of(t * prow, prow), prow), :]
@@ -594,42 +612,22 @@
         )
         post[0, :, cols] = read + skip_ref[:, cols] * din[:, cols].astype(F32)
 
+    give(dup_copies[3])
+
     @pl.when(b == 0)
     def _():
-        give(dup_copies[3])
+        join_near()
 
     @pl.when(b == 0)
     def _():
-        join_near()
-
-    @pl.when(sp == 0)
-    def _():
-        pad[pl.ds(0, 8), :] = jnp.zeros((8, cwide), F32)
-
-    in_copies[8].wait()
-
-    @pl.when(sp > 0)
-    def _():
-        tail_copy.wait_recv()
-
-    conv = jnp.zeros((rows, cwide), F32)
-    for k in range(width):
-        conv = conv + pad[pl.ds(8 + k - (width - 1), rows), :] * taps_ref[k : k + 1, :].astype(F32)
-    hc[0] = (hc[0].astype(F32) * conv).astype(BF16)
-    hc_copy = remote(hc.at[0], hc.at[1], hc_sem.at[0], hc_sem.at[1], partner)
-    hc_copy.start()
-
-    @pl.when(b > 0)
-    def _():
-        give(dup_copies[3])
-
-    for i in (0, 1):
-        pltpu.make_async_copy((so_hbm, co_hbm)[i], ov.at[i], osem.at[i]).wait()
-    oacc[...] = jnp.dot(hc[0], ov[1, :cwide], preferred_element_type=F32)
+        convolve()
+
+    pltpu.make_async_copy(ov, ov, osem.at[0]).wait()
+    oacc[...] = jnp.dot(hc[0], ov[2 * chans : 2 * chans + cwide], preferred_element_type=F32)
 
     def add_far_conv():
         hc_copy.wait_recv()
-        oacc[...] += jnp.dot(hc[1], ov[1, cwide:], preferred_element_type=F32)
+        oacc[...] += jnp.dot(hc[1], ov[2 * chans + cwide :], preferred_element_type=F32)
 
     @pl.when(b > 0)
     def _():
@@ -674,18 +672,11 @@
             cols = slice(k * LANES, (k + 1) * LANES)
             hs[slot, :, cols] = gelu(local[0, :, cols] + local[1, :, cols] * moved[k]).astype(BF16)
 
-    def far_arrival(k, c):
-        far_from = remote(
-            far_in.at[k], far_in.at[k], far_send.at[k], far_recv.at[k], {"sp": k * inner + b, "tp": 0}
-        )
-        far_from.wait_recv()
-        return c
-
     enter_copy = remote(enter.at[0], enter.at[0], enter_sem.at[0], enter_sem.at[1], partner)
 
     @pl.when(tp == 1)
     def _():
-        lax.fori_loop(0, a, far_arrival, 0)
+        wait_many(far_in, (far_sem.at[0], far_sem.at[1]), a, last, False)
         enter[0, 0], enter[0, 1] = entering(0, (aux_far[0], aux_far[1]))
         enter_copy.start()
         enter[1, 0], enter[1, 1] = entering(1, whole)
@@ -700,11 +691,11 @@
     @pl.when(tp == 1)
     def _():
         hs_copy.start()
-        for copy in dup_copies:
+        for copy in waited:
             copy.wait_recv()
         correct(0, table_far, map_far, post_far, 1)
 
-    oacc[...] += jnp.dot(hs[0], ov[0, :chans], preferred_element_type=F32)
+    oacc[...] += jnp.dot(hs[0], ov[:chans], preferred_element_type=F32)
 
     @pl.when(b == 0)
     def _():
@@ -714,7 +705,7 @@
     def _():
         hs_copy.wait_recv()
 
-    out_ref[...] = (oacc[...] + jnp.dot(hs[1], ov[0, chans:], preferred_element_type=F32)).astype(BF16)
+    out_ref[...] = (oacc[...] + jnp.dot(hs[1], ov[chans : 2 * chans], preferred_element_type=F32)).astype(BF16)
 
     x_copy.wait_send()
     hc_copy.wait_send()
@@ -727,29 +718,24 @@
     @pl.when(tp == 0)
     def _():
         aux_copy.wait_send()
-        for copy in dup_copies:
+        for copy in waited:
             copy.wait_send()
 
     @pl.when(sp < n - 1)
     def _():
         tail_copy.wait_send()
 
-    def near_sent(k, c):
-        @pl.when((k != b) | ((tp == 0) & (a < last)))
-        def _():
-            near_copy(k).wait_send()
-
-        return c
-
-    def far_sent(k, c):
-        far_copy(k).wait_send()
-        return c
-
-    lax.fori_loop(near_from, inner, near_sent, 0)
+    wait_many(
+        near_in.at[0],
+        (near_sem.at[2], near_sem.at[0]),
+        jnp.where(a < last, inner - tp, inner - 1 - b),
+        inner,
+        True,
+    )
 
     @pl.when(tp == 1)
     def _():
-        lax.fori_loop(a + 1, outer, far_sent, 0)
+        wait_many(far_in, (far_sem.at[0], far_sem.at[1]), last - a, last, True)
 
 
 def on_device(
@@ -798,7 +784,7 @@
             pltpu.VMEM(initial_state.shape, F32),
             pltpu.VMEM(conv_taps.shape, BF16),
             pltpu.VMEM((4, 2 * half, chans), BF16),
-            pltpu.VMEM((2, 2 * chans, outs), BF16),
+            pltpu.VMEM((2 * chans + 2 * cwide, outs), BF16),
             pltpu.VMEM((rows, half), BF16),
             pltpu.VMEM((rows, 2 * half), BF16),
             pltpu.VMEM((rows, chans), BF16),
@@ -832,19 +818,17 @@
             pltpu.VMEM((2, rows, cwide), BF16),
             pltpu.VMEM((rows, outs), F32),
             dma((9,)),
-            dma((5,)),
+            dma((4,)),
+            dma((1,)),
             dma((2,)),
             dma((2,)),
             dma((2,)),
             dma((2,)),
-            dma((2,)),
-            dma((inner,)),
-            dma((2, inner)),
-            dma((n // inner,)),
-            dma((n // inner,)),
+            dma((3,)),
             dma((2,)),
             dma((2,)),
-            dma((2, 4)),
+            dma((2,)),
+            dma((2, 3)),
             pltpu.SemaphoreType.REGULAR,
             pltpu.SemaphoreType.REGULAR,
         ],

time: 13.4 us -> 13 us (0.970)
  Pallas kernels: 12.4 us -> 12 us
    pallas_call x1, Pallas kernels: 12.4 us -> 12 us  [on_device(): pl.pallas_call(functools.partial(kernel, n), out_shape=pltpu.VMEM((rows,...]
where the time goes in v2:
time: 13 us; the launch traced here: 12.7 us
  Pallas kernels  12 us (92%)
  local copies, waits for them, and re-layouts  0.71 us (5%)
    pallas_call x1, Pallas kernels, on_device(): pl.pallas_call(functools.partial(kernel, n), out_shape=pltpu.VMEM((rows,...  12 us
    unnamed x1, local copies, waits for them, and re-layouts  0.71 us

profile of v2, /device:TPU:25, one launch (start us, length us, event | category | flops | bytes accessed | tf_op | source)
XLA Modules:
  0.0 12.7 jit_solution(16883944393953824706)
XLA Ops:
  0.0 12.0 %shard_map.145 = bf16[128,1024]{1,0:T(8,128)(2,1)S(1)} custom-call(bf16[128,1024]{1,0:T(8,128)(2,1)} %x_hbm.1, f32[1,2048]{1,0:T(1,128)} %bitcast.6, bf16[2048,512]{1,0:T(8,128)(2,1)} %w0_hbm.1, bf16[2048,512]{1,0:T(8,128)(2,1)} %w1_hbm.1, bf16[2048,512]{1,0:T(8,128)(2,1)} %w2_hbm.1, bf16[2048,512]{1,0:T(8,128)(2,1)} %w3_hbm.1, ...), custom_call_target="tpu_custom_call" | custom-call | tf_op jit(solution)/shard_map/pallas_call | solution.py:771
  12.0 0.7 %copy.17 = bf16[128,1024]{1,0:T(8,128)(2,1)} copy(bf16[128,1024]{1,0:T(8,128)(2,1)S(1)} %shard_map.145) | data formatting | bytes 524288

commit v3 on v2

--- a/solution.py
+++ b/solution.py
@@ -158,16 +158,15 @@
         for t in (0, 1):
             pl.semaphore_signal(sem, inc=1, device_id={"sp": j, "tp": t}, device_id_type=MESH)
 
-    def greet_near(k, c):
-        tell(barrier, a * inner + k)
-        return c
-
     def greet_far(k, c):
         tell(barrier, k * inner + b)
         return c
 
     pl.semaphore_signal(barrier, inc=1, device_id=partner, device_id_type=MESH)
-    lax.fori_loop(b + 1, inner, greet_near, 0)
+
+    @pl.when(b < inner - 1)
+    def _():
+        tell(barrier, sp + inner - 1 - b)
 
     lax.fori_loop(a + 1, outer, greet_far, 0)
 
@@ -195,7 +194,7 @@
     fetch_weight(0, 0, wsem.at[0])
     fetch_weight(0, 1, wsem.at[0])
 
-    pl.semaphore_wait(barrier, 1 + 2 * (b + a))
+    pl.semaphore_wait(barrier, 1 + 2 * (a + jnp.where(b == inner - 1, b, 0)))
 
     def ready_near(k, c):
         tell(near_ready, a * inner + k)
@@ -205,7 +204,7 @@
         tell(far_ready, k * inner + b)
         return c
 
-    @pl.when(tp == 1)
+    @pl.when((tp == 1) & (b == inner - 1))
     def _():
         lax.fori_loop(0, b, ready_near, 0)
 
@@ -379,11 +378,9 @@
 
     near_from = jnp.where(a < last, 0, b + 1)
     near_upto = jnp.where(a < last, inner, b)
-    after = inner - 1 - b
-
-    @pl.when(after > 0)
-    def _():
-        pl.semaphore_wait(near_ready, after)
+    @pl.when(b < inner - 1)
+    def _():
+        pl.semaphore_wait(near_ready, 1)
 
     def send_near(k, c):
         @pl.when((k != b) | ((tp == 0) & (a < last)))
@@ -400,13 +397,14 @@
     aux[3] = pair_up(2, twice(init_ref[1]))
     aux_copy = remote(aux, aux_far, aux_sem.at[0], aux_sem.at[1], partner)
     dup_copies = [
-        remote(src, dst, dup_sem.at[0, min(i, 2)], dup_sem.at[1, min(i, 2)], partner)
+        remote(src, dst, dup_sem.at[0, (0, 1, 2, 2, 1)[i]], dup_sem.at[1, (0, 1, 2, 2, 1)[i]], partner)
         for i, (src, dst) in enumerate(
             (
                 (tbl, table_far),
-                (map_t, map_far),
+                (map_t.at[pl.ds(0, states), :], map_far.at[pl.ds(0, states), :]),
                 (post.at[1], post_far.at[1]),
                 (post.at[0], post_far.at[0]),
+                (map_t.at[pl.ds(states, states), :], map_far.at[pl.ds(states, states), :]),
             )
         )
     ]
@@ -416,8 +414,9 @@
         def _():
             copy.start()
 
-    waited = dup_copies[:2] + [
-        remote(post, post_far, dup_sem.at[0, 2], dup_sem.at[1, 2], partner)
+    waited = [
+        remote(src, dst, dup_sem.at[0, i], dup_sem.at[1, i], partner)
+        for i, (src, dst) in enumerate(((tbl, table_far), (map_t, map_far), (post, post_far)))
     ]
 
     give(aux_copy)
@@ -482,9 +481,13 @@
         keep = lax.rem(lax.broadcasted_iota(jnp.int32, v.shape, 1), state) < state // 2
         return v + jnp.where(keep, pltpu.roll(v, LANES - state // 2, 1), pltpu.roll(v, state // 2, 1))
 
-    def unpack_all(ref, h, count, index):
-        packs = jnp.concatenate([ref[index(h, k) + (pl.ds(2 * prow, prow),)] for k in range(count)], axis=0)
-        mags_in[h, : count * prow, :] = unpacked(packs)
+    def unpack_all(ref, count, index):
+        packs = [
+            ref[index(h, k) + (pl.ds(2 * prow, prow),)] for h in (0, 1) for k in range(count)
+        ]
+        v = unpacked(jnp.concatenate(packs, axis=0))
+        for h in (0, 1):
+            mags_in[h, : count * prow, :] = v[h * count * prow : (h + 1) * count * prow]
 
     def message(ref, h, k):
         return (
@@ -497,24 +500,28 @@
         far_copy(outer + a - k).start()
         return c
 
-    def join_half(h, turned, first):
-        unpack_all(near_in, h, inner, lambda h, k: (h, k))
-
-        def near_step(k, c):
+    def join_halves(turned, first):
+        unpack_all(near_in, inner, lambda h, k: (h, k))
+
+        def half_step(h, k, c):
             ends, mag_all, phase, mine = c[0:2], c[2], c[3:5], c[5:]
             k_re, k_im, k_mag = message(near_in.at[h, k], h, k)
-            moved = cmul((turned[0] * k_mag, turned[1] * k_mag), ends)
-            now = (moved[0] + k_re, moved[1] + k_im, mag_all * k_mag) + cmul(turned, phase)
+            moved = cmul((turned[h][0] * k_mag, turned[h][1] * k_mag), ends)
+            now = (moved[0] + k_re, moved[1] + k_im, mag_all * k_mag) + cmul(turned[h], phase)
             return now + tuple(jnp.where(k < b, v, w) for v, w in zip(now, mine))
 
+        def near_step(k, c):
+            return tuple(half_step(h, k, c[h]) for h in (0, 1))
+
         one = jnp.ones((prow, LANES), F32)
-        begin = tuple(jnp.where(a == 0, v, zero) for v in first) + (one, one, zero)
-        plane = lax.fori_loop(0, near_upto, near_step, begin + begin)
-        for i in range(5):
-            held[h, i] = plane[5 + i]
-        far_out[h, pl.ds(0, prow), :] = plane[0].astype(BF16)
-        far_out[h, pl.ds(prow, prow), :] = plane[1].astype(BF16)
-        far_out[h, pl.ds(2 * prow, prow), :] = packed(plane[2])
+        begin = [tuple(jnp.where(a == 0, v, zero) for v in f) + (one, one, zero) for f in first]
+        planes = lax.fori_loop(0, near_upto, near_step, tuple(v + v for v in begin))
+        for h, plane in enumerate(planes):
+            far_out[h, pl.ds(0, prow), :] = plane[0].astype(BF16)
+            far_out[h, pl.ds(prow, prow), :] = plane[1].astype(BF16)
+            far_out[h, pl.ds(2 * prow, prow), :] = packed(plane[2])
+            for i in range(5):
+                held[h, i] = plane[5 + i]
 
     def join_near():
         @pl.when(tp == 1)
@@ -527,8 +534,9 @@
                     inner,
                     False,
                 )
-            join_half(1, whole, (aux[2], aux[3]))
-            join_half(0, (aux_far[0], aux_far[1]), (aux_far[2], aux_far[3]))
+            join_halves(
+                ((aux_far[0], aux_far[1]), whole), ((aux_far[2], aux_far[3]), (aux[2], aux[3]))
+            )
 
         @pl.when((a < last) & (b < inner - 1))
         def _():
@@ -587,6 +595,8 @@
     @pl.when(b > 0)
     def _():
         convolve()
+
+    give(dup_copies[4])
 
     def scan(t, h):
         m = mag[pl.ds(pl.multiple_of(t * prow, prow), prow), :]
@@ -601,6 +611,11 @@
         return new_re, new_im
 
     lax.fori_loop(0, rows, scan, (zero, zero), unroll=8)
+
+    @pl.when(b == 0)
+    def _():
+        join_near()
+
     for k in range(blocks):
         cols = slice(k * LANES, (k + 1) * LANES)
         at = [half_row + k * quads + q for q in range(quads) for half_row in (0, prow)]
@@ -616,10 +631,6 @@
 
     @pl.when(b == 0)
     def _():
-        join_near()
-
-    @pl.when(b == 0)
-    def _():
         convolve()
 
     pltpu.make_async_copy(ov, ov, osem.at[0]).wait()
@@ -635,8 +646,6 @@
 
     def entering(h, turned):
         plane_turn = cpow(turned, inner)
-
-        unpack_all(far_in, h, last, lambda h, k: (k, h))
 
         def far_step(k, c):
             k_re, k_im, k_mag = message(far_in.at[k, h], h, k)
@@ -668,15 +677,19 @@
                     preferred_element_type=F32,
                 )
             )
+        made = []
         for k in range(blocks):
             cols = slice(k * LANES, (k + 1) * LANES)
-            hs[slot, :, cols] = gelu(local[0, :, cols] + local[1, :, cols] * moved[k]).astype(BF16)
+            made.append(gelu(local[0, :, cols] + local[1, :, cols] * moved[k]).astype(BF16))
+            hs[slot, :, cols] = made[k]
+        return made
 
     enter_copy = remote(enter.at[0], enter.at[0], enter_sem.at[0], enter_sem.at[1], partner)
 
     @pl.when(tp == 1)
     def _():
         wait_many(far_in, (far_sem.at[0], far_sem.at[1]), a, last, False)
+        unpack_all(far_in, last, lambda h, k: (k, h))
         enter[0, 0], enter[0, 1] = entering(0, (aux_far[0], aux_far[1]))
         enter_copy.start()
         enter[1, 0], enter[1, 1] = entering(1, whole)
@@ -685,17 +698,25 @@
     def _():
         enter_copy.wait_recv()
 
-    correct(tp, tbl, map_t, post, 0)
     hs_copy = remote(hs.at[0], hs.at[1], hs_sem.at[0], hs_sem.at[1], partner)
 
+    def add_own(blks):
+        oacc[...] += jnp.dot(
+            jnp.concatenate(blks, axis=1), ov[:chans], preferred_element_type=F32
+        )
+
     @pl.when(tp == 1)
     def _():
+        correct(1, tbl, map_t, post, 0)
         hs_copy.start()
         for copy in waited:
             copy.wait_recv()
         correct(0, table_far, map_far, post_far, 1)
-
-    oacc[...] += jnp.dot(hs[0], ov[:chans], preferred_element_type=F32)
+        oacc[...] += jnp.dot(hs[0], ov[:chans], preferred_element_type=F32)
+
+    @pl.when(tp == 0)
+    def _():
+        add_own(correct(0, tbl, map_t, post, 0))
 
     @pl.when(b == 0)
     def _():

time: 13 us -> 12.8 us (0.985)
  the two profiles are of different devices: /device:TPU:25 before, /device:TPU:0 now
where the time goes in v3:
time: 12.8 us; the launch traced here: 12.7 us
  Pallas kernels  12 us (94%)
  local copies, waits for them, and re-layouts  0.71 us (6%)
    pallas_call x1, Pallas kernels, on_device(): pl.pallas_call(functools.partial(kernel, n), out_shape=pltpu.VMEM((rows,...  12 us
    unnamed x1, local copies, waits for them, and re-layouts  0.71 us

profile of v3, /device:TPU:0, one launch (start us, length us, event | category | flops | bytes accessed | tf_op | source)
XLA Modules:
  0.0 12.7 jit_solution(4918241062303977468)
XLA Ops:
  0.0 12.0 %shard_map.145 = bf16[128,1024]{1,0:T(8,128)(2,1)S(1)} custom-call(bf16[128,1024]{1,0:T(8,128)(2,1)} %x_hbm.1, f32[1,2048]{1,0:T(1,128)} %bitcast.6, bf16[2048,512]{1,0:T(8,128)(2,1)} %w0_hbm.1, bf16[2048,512]{1,0:T(8,128)(2,1)} %w1_hbm.1, bf16[2048,512]{1,0:T(8,128)(2,1)} %w2_hbm.1, bf16[2048,512]{1,0:T(8,128)(2,1)} %w3_hbm.1, ...), custom_call_target="tpu_custom_call" | custom-call | tf_op jit(solution)/shard_map/pallas_call | solution.py:792
  12.0 0.7 %copy.17 = bf16[128,1024]{1,0:T(8,128)(2,1)} copy(bf16[128,1024]{1,0:T(8,128)(2,1)S(1)} %shard_map.145) | data formatting | bytes 524288

commit v4 on v3

--- a/solution.py
+++ b/solution.py
@@ -592,7 +592,9 @@
         hc[0] = (hc[0].astype(F32) * conv).astype(BF16)
         hc_copy.start()
 
-    @pl.when(b > 0)
+    even = lax.rem(b, 2) == 0
+
+    @pl.when(jnp.logical_not(even))
     def _():
         convolve()
 
@@ -629,7 +631,7 @@
 
     give(dup_copies[3])
 
-    @pl.when(b == 0)
+    @pl.when(even)
     def _():
         convolve()
 
@@ -640,7 +642,7 @@
         hc_copy.wait_recv()
         oacc[...] += jnp.dot(hc[1], ov[2 * chans + cwide :], preferred_element_type=F32)
 
-    @pl.when(b > 0)
+    @pl.when(tp == 0)
     def _():
         add_far_conv()
 
@@ -691,12 +693,20 @@
         wait_many(far_in, (far_sem.at[0], far_sem.at[1]), a, last, False)
         unpack_all(far_in, last, lambda h, k: (k, h))
         enter[0, 0], enter[0, 1] = entering(0, (aux_far[0], aux_far[1]))
-        enter_copy.start()
+
+        @pl.when(sp > 0)
+        def _():
+            enter_copy.start()
+
         enter[1, 0], enter[1, 1] = entering(1, whole)
 
-    @pl.when(tp == 0)
+    @pl.when((tp == 0) & (sp > 0))
     def _():
         enter_copy.wait_recv()
+
+    @pl.when((tp == 0) & (sp == 0))
+    def _():
+        enter[0, 0], enter[0, 1] = aux[2], aux[3]
 
     hs_copy = remote(hs.at[0], hs.at[1], hs_sem.at[0], hs_sem.at[1], partner)
 
@@ -711,16 +721,15 @@
         hs_copy.start()
         for copy in waited:
             copy.wait_recv()
+        hc_copy.wait_recv()
         correct(0, table_far, map_far, post_far, 1)
-        oacc[...] += jnp.dot(hs[0], ov[:chans], preferred_element_type=F32)
+        oacc[...] += jnp.dot(hs[0], ov[:chans], preferred_element_type=F32) + jnp.dot(
+            hc[1], ov[2 * chans + cwide :], preferred_element_type=F32
+        )
 
     @pl.when(tp == 0)
     def _():
         add_own(correct(0, tbl, map_t, post, 0))
-
-    @pl.when(b == 0)
-    def _():
-        add_far_conv()
 
     @pl.when(tp == 0)
     def _():
@@ -734,6 +743,9 @@
     @pl.when(tp == 1)
     def _():
         hs_copy.wait_send()
+
+    @pl.when((tp == 1) & (sp > 0))
+    def _():
         enter_copy.wait_send()
 
     @pl.when(tp == 0)

time: 12.8 us -> 12.6 us (0.984)
  Pallas kernels: 12 us -> 11.7 us
    pallas_call x1, Pallas kernels: 12 us -> 11.7 us  [on_device(): pl.pallas_call(functools.partial(kernel, n), out_shape=pltpu.VMEM((rows,...]
where the time goes in v4:
time: 12.6 us; the launch traced here: 12.4 us
  Pallas kernels  11.7 us (93%)
  local copies, waits for them, and re-layouts  0.71 us (6%)
    pallas_call x1, Pallas kernels, on_device(): pl.pallas_call(functools.partial(kernel, n), out_shape=pltpu.VMEM((rows,...  11.7 us
    unnamed x1, local copies, waits for them, and re-layouts  0.71 us

profile of v4, /device:TPU:0, one launch (start us, length us, event | category | flops | bytes accessed | tf_op | source)
XLA Modules:
  0.0 12.4 jit_solution(9226010831118823330)
XLA Ops:
  0.0 11.7 %shard_map.145 = bf16[128,1024]{1,0:T(8,128)(2,1)S(1)} custom-call(bf16[128,1024]{1,0:T(8,128)(2,1)} %x_hbm.1, f32[1,2048]{1,0:T(1,128)} %bitcast.6, bf16[2048,512]{1,0:T(8,128)(2,1)} %w0_hbm.1, bf16[2048,512]{1,0:T(8,128)(2,1)} %w1_hbm.1, bf16[2048,512]{1,0:T(8,128)(2,1)} %w2_hbm.1, bf16[2048,512]{1,0:T(8,128)(2,1)} %w3_hbm.1, ...), custom_call_target="tpu_custom_call" | custom-call | tf_op jit(solution)/shard_map/pallas_call | solution.py:804
  11.7 0.7 %copy.17 = bf16[128,1024]{1,0:T(8,128)(2,1)} copy(bf16[128,1024]{1,0:T(8,128)(2,1)S(1)} %shard_map.145) | data formatting | bytes 524288

commit v5 on v4

--- a/solution.py
+++ b/solution.py
@@ -211,6 +211,8 @@
 
     lax.fori_loop(0, a, ready_far, 0)
 
+    bd_in[...] = jnp.zeros_like(bd_in)
+    bd_out[...] = jnp.zeros_like(bd_out)
     when = lax.broadcasted_iota(jnp.int32, (rows, 2 * rows), 0)
     upto = lax.broadcasted_iota(jnp.int32, (rows, 2 * rows), 1)
     sums[...] = jnp.where(
@@ -297,7 +299,6 @@
             odd = cmul(odd, sixteen)
 
     def spread_map(src, dst):
-        dst[...] = jnp.zeros_like(dst)
         for b in range(blocks):
             for q in range(quads):
                 g = b * per_block + 2 * q
@@ -592,7 +593,7 @@
         hc[0] = (hc[0].astype(F32) * conv).astype(BF16)
         hc_copy.start()
 
-    even = lax.rem(b, 2) == 0
+    even = (lax.rem(b, 2) == 0) & (sp > 0)
 
     @pl.when(jnp.logical_not(even))
     def _():

time: 12.6 us -> 12.3 us (0.976)
  Pallas kernels: 11.7 us -> 11.5 us
    pallas_call x1, Pallas kernels: 11.7 us -> 11.5 us  [on_device(): pl.pallas_call(functools.partial(kernel, n), out_shape=pltpu.VMEM((rows,...]
where the time goes in v5:
time: 12.3 us; the launch traced here: 12.2 us
  Pallas kernels  11.5 us (93%)
  local copies, waits for them, and re-layouts  0.71 us (6%)
    pallas_call x1, Pallas kernels, on_device(): pl.pallas_call(functools.partial(kernel, n), out_shape=pltpu.VMEM((rows,...  11.5 us
    unnamed x1, local copies, waits for them, and re-layouts  0.71 us

profile of v5, /device:TPU:0, one launch (start us, length us, event | category | flops | bytes accessed | tf_op | source)
XLA Modules:
  0.0 12.2 jit_solution(4151152839425249875)
XLA Ops:
  0.0 11.5 %shard_map.145 = bf16[128,1024]{1,0:T(8,128)(2,1)S(1)} custom-call(bf16[128,1024]{1,0:T(8,128)(2,1)} %x_hbm.1, f32[1,2048]{1,0:T(1,128)} %bitcast.6, bf16[2048,512]{1,0:T(8,128)(2,1)} %w0_hbm.1, bf16[2048,512]{1,0:T(8,128)(2,1)} %w1_hbm.1, bf16[2048,512]{1,0:T(8,128)(2,1)} %w2_hbm.1, bf16[2048,512]{1,0:T(8,128)(2,1)} %w3_hbm.1, ...), custom_call_target="tpu_custom_call" | custom-call | tf_op jit(solution)/shard_map/pallas_call | solution.py:805
  11.5 0.7 %copy.17 = bf16[128,1024]{1,0:T(8,128)(2,1)} copy(bf16[128,1024]{1,0:T(8,128)(2,1)S(1)} %shard_map.145) | data formatting | bytes 524288

commit v6 on v5

--- a/solution.py
+++ b/solution.py
@@ -281,22 +281,28 @@
         for i in (0, 1):
             powers[i, pl.ds(k * prow, prow), :] = step[i]
         step = cmul(step, turn) if k < 7 else step
-    far_step16 = cmul(step, step)
-    for i in (0, 1):
-        powers[i, pl.ds(8 * prow, prow), :] = far_step16[i]
+    sixteen = cmul(step, step)
+    leap = sixteen
+    for k in range(rows // 16 - 1):
+        for i in (0, 1):
+            powers[i, pl.ds((8 + k) * prow, prow), :] = leap[i]
+        leap = cmul(leap, sixteen)
     whole = cpow(step, rows // 8)
     for r in range(prow):
         even = [powers[i, pl.ds(r, 8, stride=prow), :] for i in (0, 1)]
         eight = [powers[i, pl.ds(7 * prow + r, 1), :] for i in (0, 1)]
-        sixteen = [powers[i, pl.ds(8 * prow + r, 1), :] for i in (0, 1)]
         odd = cmul(even, eight)
+        base = [jnp.concatenate([even[i], odd[i]], axis=0).astype(BF16) for i in (0, 1)]
         for t in range(0, rows, 16):
+            now = base
+            if t > 0:
+                at = pl.ds((8 + t // 16 - 1) * prow + r, 1)
+                now = cmul(
+                    base,
+                    [jnp.broadcast_to(powers[i, at, :], (16, LANES)).astype(BF16) for i in (0, 1)],
+                )
             for i in (0, 1):
-                tbl[t : t + 16, (2 * r + i) * LANES : (2 * r + i + 1) * LANES] = jnp.concatenate(
-                    [even[i], odd[i]], axis=0
-                ).astype(BF16)
-            even = cmul(even, sixteen)
-            odd = cmul(odd, sixteen)
+                tbl[t : t + 16, (2 * r + i) * LANES : (2 * r + i + 1) * LANES] = now[i]
 
     def spread_map(src, dst):
         for b in range(blocks):
@@ -826,7 +832,7 @@
             pltpu.VMEM((chans, bdw), BF16),
             pltpu.VMEM((2 * states, LANES), BF16),
             pltpu.VMEM((rows, 2 * states), BF16),
-            pltpu.VMEM((2, 9 * prow, LANES), F32),
+            pltpu.VMEM((2, (8 + rows // 16) * prow, LANES), F32),
             pltpu.VMEM((rows, chans), F32),
             pltpu.VMEM((rows, chans), F32),
             pltpu.VMEM((2, prow, LANES), F32),

time: 12.3 us -> 12.3 us (level)
  no operation moved by 1% of the time
where the time goes in v6:
time: 12.3 us; the launch traced here: 12.2 us
  Pallas kernels  11.5 us (93%)
  local copies, waits for them, and re-layouts  0.71 us (6%)
    pallas_call x1, Pallas kernels, on_device(): pl.pallas_call(functools.partial(kernel, n), out_shape=pltpu.VMEM((rows,...  11.5 us
    unnamed x1, local copies, waits for them, and re-layouts  0.71 us

profile of v6, /device:TPU:0, one launch (start us, length us, event | category | flops | bytes accessed | tf_op | source)
XLA Modules:
  0.0 12.2 jit_solution(18310754834315536622)
XLA Ops:
  0.0 11.5 %shard_map.145 = bf16[128,1024]{1,0:T(8,128)(2,1)S(1)} custom-call(bf16[128,1024]{1,0:T(8,128)(2,1)} %x_hbm.1, f32[1,2048]{1,0:T(1,128)} %bitcast.6, bf16[2048,512]{1,0:T(8,128)(2,1)} %w0_hbm.1, bf16[2048,512]{1,0:T(8,128)(2,1)} %w1_hbm.1, bf16[2048,512]{1,0:T(8,128)(2,1)} %w2_hbm.1, bf16[2048,512]{1,0:T(8,128)(2,1)} %w3_hbm.1, ...), custom_call_target="tpu_custom_call" | custom-call | tf_op jit(solution)/shard_map/pallas_call | solution.py:811
  11.5 0.7 %copy.17 = bf16[128,1024]{1,0:T(8,128)(2,1)} copy(bf16[128,1024]{1,0:T(8,128)(2,1)S(1)} %shard_map.145) | data formatting | bytes 524288

commit v7 on v6

--- a/solution.py
+++ b/solution.py
@@ -598,6 +598,8 @@
             conv = conv + pad[pl.ds(8 + k - (width - 1), rows), :] * taps_ref[k : k + 1, :].astype(F32)
         hc[0] = (hc[0].astype(F32) * conv).astype(BF16)
         hc_copy.start()
+        pltpu.make_async_copy(ov, ov, osem.at[0]).wait()
+        oacc[...] = jnp.dot(hc[0], ov[2 * chans : 2 * chans + cwide], preferred_element_type=F32)
 
     even = (lax.rem(b, 2) == 0) & (sp > 0)
 
@@ -642,8 +644,6 @@
     def _():
         convolve()
 
-    pltpu.make_async_copy(ov, ov, osem.at[0]).wait()
-    oacc[...] = jnp.dot(hc[0], ov[2 * chans : 2 * chans + cwide], preferred_element_type=F32)
 
     def add_far_conv():
         hc_copy.wait_recv()

time: 12.3 us -> 12.3 us (level)
  the two profiles are of different devices: /device:TPU:0 before, /device:TPU:17 now
where the time goes in v7:
time: 12.3 us; the launch traced here: 12.2 us
  Pallas kernels  11.5 us (93%)
  local copies, waits for them, and re-layouts  0.71 us (6%)
    pallas_call x1, Pallas kernels, on_device(): pl.pallas_call(functools.partial(kernel, n), out_shape=pltpu.VMEM((rows,...  11.5 us
    unnamed x1, local copies, waits for them, and re-layouts  0.71 us

profile of v7, /device:TPU:17, one launch (start us, length us, event | category | flops | bytes accessed | tf_op | source)
XLA Modules:
  0.0 12.2 jit_solution(7244409152563649892)
XLA Ops:
  0.0 11.5 %shard_map.145 = bf16[128,1024]{1,0:T(8,128)(2,1)S(1)} custom-call(bf16[128,1024]{1,0:T(8,128)(2,1)} %x_hbm.1, f32[1,2048]{1,0:T(1,128)} %bitcast.6, bf16[2048,512]{1,0:T(8,128)(2,1)} %w0_hbm.1, bf16[2048,512]{1,0:T(8,128)(2,1)} %w1_hbm.1, bf16[2048,512]{1,0:T(8,128)(2,1)} %w2_hbm.1, bf16[2048,512]{1,0:T(8,128)(2,1)} %w3_hbm.1, ...), custom_call_target="tpu_custom_call" | custom-call | tf_op jit(solution)/shard_map/pallas_call | solution.py:811
  11.5 0.7 %copy.17 = bf16[128,1024]{1,0:T(8,128)(2,1)} copy(bf16[128,1024]{1,0:T(8,128)(2,1)S(1)} %shard_map.145) | data formatting | bytes 524288
